TPU v7x, 32 devices: a whole 2x2x4 slice. The times are simulated.
32 devices in a mesh: fs: 8 (over z, core), tp: 4 (over y, x).
Axes of the slice: x: 2, y: 2, z: 4, core: 2. Of those that a mesh axis runs over, the one named last changes fastest.
Arguments:
- late_input: bfloat16 [1024, 2048], P('fs'), may hold values from -6 to 6
- early_input: bfloat16 [1024, 2048], P('fs'), may hold values from -6 to 6
- early_mid: bfloat16 [1024, 2048], P('fs'), may hold values from -6 to 6
- cotangent: bfloat16 [1024, 2048], P('fs'), may hold values from -6 to 6
- gain_first: float32 [2048], replicated, may hold values from 0.1 to 1.9
- gain_second: float32 [2048], replicated, may hold values from 0.1 to 1.9
- gate_first: bfloat16 [2048, 2816], P('fs', 'tp'), may hold values from -0.125 to 0.125
- up_first: bfloat16 [2048, 2816], P('fs', 'tp'), may hold values from -0.125 to 0.125
- down_first: bfloat16 [2816, 2048], P('tp', 'fs'), may hold values from -0.109375 to 0.109375
- gate_second: bfloat16 [2048, 2816], P('fs', 'tp'), may hold values from -0.125 to 0.125
- up_second: bfloat16 [2048, 2816], P('fs', 'tp'), may hold values from -0.125 to 0.125
- down_second: bfloat16 [2816, 2048], P('tp', 'fs'), may hold values from -0.109375 to 0.109375
- sum_gate_first: float32 [2048, 2816], P('fs', 'tp'), may hold values from -128 to 128
- sum_up_first: float32 [2048, 2816], P('fs', 'tp'), may hold values from -128 to 128
- sum_down_first: float32 [2816, 2048], P('tp', 'fs'), may hold values from -128 to 128
- sum_gate_second: float32 [2048, 2816], P('fs', 'tp'), may hold values from -128 to 128
- sum_up_second: float32 [2048, 2816], P('fs', 'tp'), may hold values from -128 to 128
- sum_down_second: float32 [2816, 2048], P('tp', 'fs'), may hold values from -128 to 128
Outputs:
- late_mid: bfloat16 [1024, 2048], P('fs')
- late_out: bfloat16 [1024, 2048], P('fs')
- input_grad: bfloat16 [1024, 2048], P('fs')
- new_gate_first: float32 [2048, 2816], P('fs', 'tp')
- new_up_first: float32 [2048, 2816], P('fs', 'tp')
- new_down_first: float32 [2816, 2048], P('tp', 'fs')
- new_gate_second: float32 [2048, 2816], P('fs', 'tp')
- new_up_second: float32 [2048, 2816], P('fs', 'tp')
- new_down_second: float32 [2816, 2048], P('tp', 'fs')
All inputs are finite; a program needn't handle non-finite values.
Results may differ from a plain program's by a relative error of at most 0.015.
Values may be sent and summed in bfloat16 or wider, within the bound.
A program may use at most 128 MiB of HBM per device.

v0:
```python
import jax
import jax.numpy as jnp
from jax import lax
from jax.sharding import PartitionSpec as P

norm_eps = 1e-06


def normalize(values, gain_vector):
    widened = values.astype(jnp.float32)
    factor = lax.rsqrt(jnp.mean(widened * widened, axis=-1, keepdims=True) + norm_eps)
    normed = (widened * factor * gain_vector).astype(jnp.bfloat16)
    return (widened, factor, normed)


def block_forward(values, params):
    gain_vector, w_gate, w_up, w_down = params
    widened, factor, normed = normalize(values, gain_vector)
    gate_pre = jnp.dot(normed, w_gate, preferred_element_type=jnp.float32)
    up_pre = jnp.dot(normed, w_up, preferred_element_type=jnp.float32)
    hidden = (jax.nn.silu(gate_pre) * up_pre).astype(jnp.bfloat16)
    branch = lax.psum(
        jnp.dot(hidden, w_down, preferred_element_type=jnp.float32).astype(jnp.bfloat16), "tp"
    ).astype(jnp.float32)
    return (widened + 0.5 * branch).astype(jnp.bfloat16)


def block_backward(values, cotangent, params):
    gain_vector, w_gate, w_up, w_down = params
    widened, factor, normed = normalize(values, gain_vector)
    gate_pre = jnp.dot(normed, w_gate, preferred_element_type=jnp.float32)
    up_pre = jnp.dot(normed, w_up, preferred_element_type=jnp.float32)
    sigmoid_gate = jax.nn.sigmoid(gate_pre)
    activated = gate_pre * sigmoid_gate
    hidden = (activated * up_pre).astype(jnp.bfloat16)
    hidden_grad = 0.5 * jnp.einsum(
        "td,fd->tf", cotangent, w_down, preferred_element_type=jnp.float32
    )
    gate_grad = (
        hidden_grad * up_pre * sigmoid_gate * (1.0 + gate_pre * (1.0 - sigmoid_gate))
    ).astype(jnp.bfloat16)
    up_grad = (hidden_grad * activated).astype(jnp.bfloat16)
    partial_value = jnp.einsum("tf,df->td", gate_grad, w_gate, preferred_element_type=jnp.float32)
    partial_value = partial_value + jnp.einsum(
        "tf,df->td", up_grad, w_up, preferred_element_type=jnp.float32
    )
    normed_grad = lax.psum(partial_value.astype(jnp.bfloat16), "tp").astype(jnp.float32)
    scaled = normed_grad * gain_vector
    unit_rows = widened * factor
    rows_grad = cotangent.astype(jnp.float32) + factor * (
        scaled - unit_rows * jnp.mean(scaled * unit_rows, axis=-1, keepdims=True)
    )
    return (rows_grad, (normed, cotangent, gate_grad, up_grad, hidden))


def fold_pair(pieces, columns_in):
    return (
        jnp.einsum("td,tf->df", columns_in, pieces[0], preferred_element_type=jnp.float32),
        jnp.einsum("td,tf->df", columns_in, pieces[1], preferred_element_type=jnp.float32),
    )


def fold_block(pieces, columns_in, columns_out):
    paired = fold_pair(pieces[0:2], columns_in)
    return paired + (
        jnp.einsum("tf,td->fd", pieces[2], columns_out, preferred_element_type=jnp.float32),
    )


def per_device(
    late_input,
    early_input,
    early_mid,
    cotangent,
    gain_first,
    gain_second,
    gate_first,
    up_first,
    down_first,
    gate_second,
    up_second,
    down_second,
    sum_gate_first,
    sum_up_first,
    sum_down_first,
    sum_gate_second,
    sum_up_second,
    sum_down_second,
):
    rows_in = (
        lax.all_gather(gate_first, "fs", axis=0, tiled=True),
        lax.all_gather(up_first, "fs", axis=0, tiled=True),
        lax.all_gather(gate_second, "fs", axis=0, tiled=True),
        lax.all_gather(up_second, "fs", axis=0, tiled=True),
    )
    cols_out = (
        lax.all_gather(down_first, "fs", axis=1, tiled=True),
        lax.all_gather(down_second, "fs", axis=1, tiled=True),
    )
    first_params = (gain_first, rows_in[0], rows_in[1], cols_out[0])
    second_params = (gain_second, rows_in[2], rows_in[3], cols_out[1])
    late_mid = block_forward(late_input, first_params)
    late_out = block_forward(late_mid, second_params)

    def collect(saved_parts):
        normed, cotan_rows, gate_grad, up_grad, hidden = saved_parts
        columns_in, columns_out = (
            lax.all_to_all(normed, "fs", split_axis=1, concat_axis=0, tiled=True),
            lax.all_to_all(cotan_rows, "fs", split_axis=1, concat_axis=0, tiled=True),
        )
        result = fold_block(
            (
                lax.all_gather(gate_grad, "fs", axis=0, tiled=True),
                lax.all_gather(up_grad, "fs", axis=0, tiled=True),
                lax.all_gather(hidden, "fs", axis=0, tiled=True),
            ),
            columns_in,
            columns_out,
        )
        return (result[0], result[1], 0.5 * result[2])

    mid_grad, saved_second = block_backward(early_mid, cotangent, second_params)
    mid_grad = mid_grad.astype(jnp.bfloat16)
    grads_second = collect(saved_second)
    rows_grad, saved_first = block_backward(early_input, mid_grad, first_params)
    grads_first = collect(saved_first)
    return (
        late_mid,
        late_out,
        rows_grad.astype(jnp.bfloat16),
        sum_gate_first + grads_first[0],
        sum_up_first + grads_first[1],
        sum_down_first + grads_first[2],
        sum_gate_second + grads_second[0],
        sum_up_second + grads_second[1],
        sum_down_second + grads_second[2],
    )


def solution(mesh):
    in_specs = (
        P("fs", None),
        P("fs", None),
        P("fs", None),
        P("fs", None),
        P(),
        P(),
        P("fs", "tp"),
        P("fs", "tp"),
        P("tp", "fs"),
        P("fs", "tp"),
        P("fs", "tp"),
        P("tp", "fs"),
        P("fs", "tp"),
        P("fs", "tp"),
        P("tp", "fs"),
        P("fs", "tp"),
        P("fs", "tp"),
        P("tp", "fs"),
    )
    out_specs = (
        P("fs", None),
        P("fs", None),
        P("fs", None),
        P("fs", "tp"),
        P("fs", "tp"),
        P("tp", "fs"),
        P("fs", "tp"),
        P("fs", "tp"),
        P("tp", "fs"),
    )
    return jax.shard_map(
        per_device, mesh=mesh, in_specs=in_specs, out_specs=out_specs, check_vma=False
    )
```

profile of v0, /device:TPU:9, one launch (start us, length us, event | category | flops | bytes accessed | tf_op | source)
XLA Modules:
  0.0 554.4 jit_solution(9023970974551871583)
XLA Ops:
  11.2 1.3 fusion.18
  13.0 33.9 %all-gather.19.cloned.1.call-done = bf16[2048,704]{0,1:T(8,128)(2,1)} async-done(((bf16[256,704]{0,1:T(8,128)(2,1)}), bf16[2048,704]{0,1:T(8,128)(2,1)}) %all-gather.19.cloned.1.call-update) | async-done | bytes 2883600 | tf_op jit(solution)/shard_map/all_gather | solution.py:93
  46.8 3.5 fusion.59
  50.3 33.4 %all-gather.23.cloned.1.call-done = bf16[704,2048]{1,0:T(8,128)(2,1)} async-done(((bf16[704,256]{1,0:T(8,128)(2,1)}), bf16[704,2048]{1,0:T(8,128)(2,1)}) %all-gather.23.cloned.1.call-update) | async-done | bytes 2883600 | tf_op jit(solution)/shard_map/all_gather | solution.py:98
  83.7 3.5 convolution_multiply_fusion.3
  87.2 33.4 %all-gather.13.cloned.1.call-done = bf16[2048,704]{0,1:T(8,128)(2,1)} async-done(((bf16[256,704]{0,1:T(8,128)(2,1)}), bf16[2048,704]{0,1:T(8,128)(2,1)}) %all-gather.13.cloned.1.call-update) | async-done | bytes 2883600 | tf_op jit(solution)/shard_map/all_gather | solution.py:91
  120.6 3.5 fusion.54
  124.1 33.2 %all-gather.21.cloned.1.call-done = bf16[2048,704]{0,1:T(8,128)(2,1)} async-done(((bf16[256,704]{0,1:T(8,128)(2,1)}), bf16[2048,704]{0,1:T(8,128)(2,1)}) %all-gather.21.cloned.1.call-update) | async-done | bytes 2883600 | tf_op jit(solution)/shard_map/all_gather | solution.py:94
  157.3 3.8 multiply_convert_fusion
  161.1 2.5 fusion.60
  163.6 3.7 fusion
  167.3 26.7 %all-gather.15.cloned.1.call-done = bf16[2048,704]{0,1:T(8,128)(2,1)} async-done(((bf16[256,704]{0,1:T(8,128)(2,1)}), bf16[2048,704]{0,1:T(8,128)(2,1)}) %all-gather.15.cloned.1.call-update) | async-done | bytes 2883600 | tf_op jit(solution)/shard_map/all_gather | solution.py:92
  194.0 36.7 %all-gather.17.cloned.1.call-done = bf16[704,2048]{1,0:T(8,128)(2,1)} async-done(((bf16[704,256]{1,0:T(8,128)(2,1)}), bf16[704,2048]{1,0:T(8,128)(2,1)}) %all-gather.17.cloned.1.call-update) | async-done | bytes 2883600 | tf_op jit(solution)/shard_map/all_gather | solution.py:97
  230.7 6.0 %convolution_convert_fusion.1 = bf16[128,2048]{1,0:T(8,128)(2,1)} fusion(bf16[704,2048]{1,0:T(8,128)(2,1)} %all-gather.17.cloned.1.call-done, bf16[2048,704]{0,1:T(8,128)(2,1)} %all-gather.15.cloned.1.call-done, f32[128,704]{0,1:T(8,128)} %fusion.54, bf16[128,2048]{1,0:T(8,128)(2,1)} %param.18, f32[2048]{0:T(1024)S(1)} %copy-done.23, f32[128]{0:T(128)S(1)} %add_rsqrt_fusion.3), kind=kOutput, calls=%fused_computation.5 | convolution fusion | flops 740048896 | bytes 7184896 | tf_op jit(solution)/shard_map/dot_general | solution.py:23
  236.9 1.2 fusion.25
  238.2 1.2 fusion.19
  240.2 3.5 fusion.61
  243.7 44.7 %all-reduce.7.cloned.1.call-done = (bf16[128,2048]{1,0:T(8,128)(2,1)}, bf16[128,2048]{1,0:T(8,128)(2,1)}) async-done(((bf16[128,2048]{1,0:T(8,128)(2,1)}, bf16[128,2048]{1,0:T(8,128)(2,1)}), (bf16[128,2048]{1,0:T(8,128)(2,1)}, bf16[128,2048]{1,0:T(8,128)(2,1)})) %all-reduce.7.cloned.1.call-update) | async-done | bytes 1048592 | tf_op jit(solution)/shard_map/psum | solution.py:22
  288.3 1.5 fusion.13
  289.9 1.6 fusion.17
  291.5 1.7 fusion.30
  294.2 1.7 multiply_convert_fusion.1
  296.0 3.6 fusion.62
  299.6 1.7 fusion.50
  301.3 6.0 %convolution_convert_fusion = bf16[128,2048]{1,0:T(8,128)(2,1)} fusion(bf16[704,2048]{1,0:T(8,128)(2,1)} %all-gather.23.cloned.1.call-done, bf16[2048,704]{0,1:T(8,128)(2,1)} %all-gather.21.cloned.1.call-done, f32[128,704]{0,1:T(8,128)} %fusion.50, bf16[128,2048]{1,0:T(8,128)(2,1)S(1)} %get-tuple-element.14, f32[2048]{0:T(1024)S(1)} %copy-done.22, ...), kind=kOutput, calls=%fused_computation.4 | convolution fusion | flops 740048896 | bytes 7184896 | tf_op jit(solution)/shard_map/dot_general | solution.py:23
  307.3 2.7 fusion.1
  313.4 2.0 copy.33
  315.5 5.7 %all-to-all-start.3 = ((bf16[128,8,256]{0,2,1:T(8,128)(2,1)}), bf16[128,8,256]{0,2,1:T(8,128)(2,1)S(1)}, u32[]{:S(2)}, u32[]{:S(2)}) async-start(bf16[128,8,256]{0,2,1:T(8,128)(2,1)} %bitcast.8), calls=%async_computation.3 | async-start | bytes 1048576 | tf_op jit(solution)/shard_map/all_to_all | solution.py:109
  322.0 11.0 %all-to-all-done.3 = bf16[128,8,256]{0,2,1:T(8,128)(2,1)S(1)} async-done(((bf16[128,8,256]{0,2,1:T(8,128)(2,1)}), bf16[128,8,256]{0,2,1:T(8,128)(2,1)S(1)}, u32[]{:S(2)}, u32[]{:S(2)}) %all-to-all-start.3) | async-done | bytes 524320 | tf_op jit(solution)/shard_map/all_to_all | solution.py:109
  333.0 6.9 %all-to-all-start.2 = ((bf16[128,8,256]{2,0,1:T(8,128)(2,1)}), bf16[128,8,256]{2,0,1:T(8,128)(2,1)S(1)}, u32[]{:S(2)}, u32[]{:S(2)}) async-start(bf16[128,8,256]{2,0,1:T(8,128)(2,1)} %bitcast.59), calls=%async_computation.2 | async-start | bytes 1048576 | tf_op jit(solution)/shard_map/all_to_all | solution.py:108
  341.8 20.8 %all-reduce.5.cloned.1.call-done = (bf16[128,2048]{1,0:T(8,128)(2,1)}, bf16[128,2048]{1,0:T(8,128)(2,1)}) async-done(((bf16[128,2048]{1,0:T(8,128)(2,1)}, bf16[128,2048]{1,0:T(8,128)(2,1)}), (bf16[128,2048]{1,0:T(8,128)(2,1)}, bf16[128,2048]{1,0:T(8,128)(2,1)})) %all-reduce.5.cloned.1.call-update) | async-done | bytes 1048592 | tf_op jit(solution)/shard_map/psum | solution.py:22
  362.6 1.4 fusion.20
  364.1 2.3 fusion.24
  366.3 5.6 %all-to-all-start = ((bf16[128,8,256]{2,0,1:T(8,128)(2,1)}), bf16[128,8,256]{2,0,1:T(8,128)(2,1)S(1)}, u32[]{:S(2)}, u32[]{:S(2)}) async-start(bf16[128,8,256]{2,0,1:T(8,128)(2,1)} %bitcast.61), calls=%async_computation | async-start | bytes 1048576 | tf_op jit(solution)/shard_map/all_to_all | solution.py:108
  371.9 2.0 fusion.33
  373.9 27.7 %all-gather.33.cloned.1.call-done = bf16[1024,704]{0,1:T(8,128)(2,1)} async-done(((bf16[128,704]{0,1:T(8,128)(2,1)}), bf16[1024,704]{0,1:T(8,128)(2,1)}) %all-gather.33.cloned.1.call-update) | async-done | bytes 1441808 | tf_op jit(solution)/shard_map/all_gather | solution.py:114
  401.7 2.8 convolution_add_fusion.2
  404.4 25.2 %all-gather.31.cloned.1.call-done = bf16[1024,704]{0,1:T(8,128)(2,1)} async-done(((bf16[128,704]{0,1:T(8,128)(2,1)}), bf16[1024,704]{0,1:T(8,128)(2,1)}) %all-gather.31.cloned.1.call-update) | async-done | bytes 1441808 | tf_op jit(solution)/shard_map/all_gather | solution.py:113
  429.6 2.9 convolution_add_fusion.3
  432.6 3.6 all-to-all-start.1
  436.2 29.4 %all-gather.35.cloned.1.call-done = bf16[1024,704]{0,1:T(8,128)(2,1)} async-done(((bf16[128,704]{0,1:T(8,128)(2,1)}), bf16[1024,704]{0,1:T(8,128)(2,1)}) %all-gather.35.cloned.1.call-update) | async-done | bytes 1441808 | tf_op jit(solution)/shard_map/all_gather | solution.py:115
  465.5 2.8 fusion.8
  468.3 23.7 %all-gather.27.cloned.1.call-done = bf16[1024,704]{0,1:T(8,128)(2,1)} async-done(((bf16[128,704]{0,1:T(8,128)(2,1)}), bf16[1024,704]{0,1:T(8,128)(2,1)}) %all-gather.27.cloned.1.call-update) | async-done | bytes 1441808 | tf_op jit(solution)/shard_map/all_gather | solution.py:114
  492.0 2.8 convolution_add_fusion.4
  494.9 23.8 %all-gather.25.cloned.1.call-done = bf16[1024,704]{0,1:T(8,128)(2,1)} async-done(((bf16[128,704]{0,1:T(8,128)(2,1)}), bf16[1024,704]{0,1:T(8,128)(2,1)}) %all-gather.25.cloned.1.call-update) | async-done | bytes 1441808 | tf_op jit(solution)/shard_map/all_gather | solution.py:113
  518.7 2.8 convolution_add_fusion.5
  521.4 23.7 %all-gather.29.cloned.1.call-done = bf16[1024,704]{0,1:T(8,128)(2,1)} async-done(((bf16[128,704]{0,1:T(8,128)(2,1)}), bf16[1024,704]{0,1:T(8,128)(2,1)}) %all-gather.29.cloned.1.call-update) | async-done | bytes 1441808 | tf_op jit(solution)/shard_map/all_gather | solution.py:115
  545.1 2.8 fusion.9
  (92 shorter events, 12.4 us)
Async XLA Ops:
  7.2 5.5 copy-start.5
  7.2 5.3 copy-start.6
  7.2 5.5 copy-start.22
  7.2 39.6 %all-gather.19.cloned.1.call-start = ((), (), s32[]{:S(2)}) async-start(), calls=%async_computation.7 | async-start | bytes 3244032 | tf_op jit(solution)/shard_map/all_gather | solution.py:93
  7.9 75.8 %all-gather.23.cloned.1.call-start = ((), (), s32[]{:S(2)}) async-start(), calls=%async_computation.9 | async-start | bytes 3244032 | tf_op jit(solution)/shard_map/all_gather | solution.py:98
  8.7 111.9 %all-gather.13.cloned.1.call-start = ((), (), s32[]{:S(2)}) async-start(), calls=%async_computation.4 | async-start | bytes 3244032 | tf_op jit(solution)/shard_map/all_gather | solution.py:91
  9.4 147.8 %all-gather.21.cloned.1.call-start = ((), (), s32[]{:S(2)}) async-start(), calls=%async_computation.8 | async-start | bytes 3244032 | tf_op jit(solution)/shard_map/all_gather | solution.py:94
  10.0 184.0 %all-gather.15.cloned.1.call-start = ((), (), s32[]{:S(2)}) async-start(), calls=%async_computation.5 | async-start | bytes 3244032 | tf_op jit(solution)/shard_map/all_gather | solution.py:92
  10.6 220.1 %all-gather.17.cloned.1.call-start = ((), (), s32[]{:S(2)}) async-start(), calls=%async_computation.6 | async-start | bytes 3244032 | tf_op jit(solution)/shard_map/all_gather | solution.py:97
  11.2 72.5 %copy-start.15 = (bf16[128,2048]{1,0:T(8,128)(2,1)S(1)}, bf16[128,2048]{1,0:T(8,128)(2,1)}, u32[]{:S(2)}) copy-start(bf16[128,2048]{1,0:T(8,128)(2,1)} %param.21) | copy-start | bytes 1572868
  11.2 277.2 %all-reduce.7.cloned.1.call-start = ((), (), s32[]{:S(2)}) async-start(), calls=%async_computation.17 | async-start | bytes 2097152 | tf_op jit(solution)/shard_map/psum | solution.py:22
  12.9 74.2 %copy-start.10 = (bf16[128,2048]{1,0:T(8,128)(2,1)}, bf16[128,2048]{1,0:T(8,128)(2,1)S(1)}, u32[]{:S(2)}) copy-start(bf16[128,2048]{1,0:T(8,128)(2,1)S(1)} %fusion.12) | copy-start | bytes 1572868
  12.9 107.6 %copy-start.23 = (f32[2048]{0:T(1024)S(1)}, f32[2048]{0:T(1024)}, u32[]{:S(2)}) copy-start(f32[2048]{0:T(1024)} %param.22) | copy-start | bytes 24580
  124.1 37.0 %copy-start = (bf16[2048,704]{0,1:T(8,128)(2,1)S(1)}, bf16[2048,704]{0,1:T(8,128)(2,1)}, u32[]{:S(2)}) copy-start(bf16[2048,704]{0,1:T(8,128)(2,1)} %all-gather.19.cloned.1.call-done) | copy-start | bytes 8650756
  236.7 125.9 %all-reduce.5.cloned.1.call-start = ((), (), s32[]{:S(2)}) async-start(), calls=%async_computation.16 | async-start | bytes 2097152 | tf_op jit(solution)/shard_map/psum | solution.py:22
  239.4 0.8 copy-start.12
  288.3 5.0 copy-start.3
  291.5 1.8 copy-start.8
  291.5 2.7 copy-start.1
  291.5 2.7 copy-start.13
  291.5 2.7 copy-start.21
  293.3 78.7 %copy-start.4 = (bf16[128,2048]{1,0:T(8,128)(2,1)}, bf16[128,2048]{1,0:T(8,128)(2,1)S(1)}, u32[]{:S(2)}) copy-start(bf16[128,2048]{1,0:T(8,128)(2,1)S(1)} %get-tuple-element.14) | copy-start | bytes 1572868
  301.3 6.0 %copy-start.2 = (bf16[2048,704]{0,1:T(8,128)(2,1)S(1)}, bf16[2048,704]{0,1:T(8,128)(2,1)}, u32[]{:S(2)}) copy-start(bf16[2048,704]{0,1:T(8,128)(2,1)} %all-gather.15.cloned.1.call-done) | copy-start | bytes 8650756
  310.0 11.2 %copy-start.11 = (bf16[128,2048]{1,0:T(8,128)(2,1)S(1)}, bf16[128,2048]{1,0:T(8,128)(2,1)}, u32[]{:S(2)}) copy-start(bf16[128,2048]{1,0:T(8,128)(2,1)} %copy-done.10) | copy-start | bytes 1572868
  310.0 29.9 %copy-start.14 = (bf16[128,2048]{1,0:T(8,128)(2,1)S(1)}, bf16[128,2048]{1,0:T(8,128)(2,1)}, u32[]{:S(2)}) copy-start(bf16[128,2048]{1,0:T(8,128)(2,1)} %copy-done.12) | copy-start | bytes 1572868
  310.0 91.6 %all-gather.33.cloned.1.call-start = ((), (), s32[]{:S(2)}) async-start(), calls=%async_computation.14 | async-start | bytes 1622016 | tf_op jit(solution)/shard_map/all_gather | solution.py:114
  310.8 118.9 %all-gather.31.cloned.1.call-start = ((), (), s32[]{:S(2)}) async-start(), calls=%async_computation.13 | async-start | bytes 1622016 | tf_op jit(solution)/shard_map/all_gather | solution.py:113
  311.4 154.2 %all-gather.35.cloned.1.call-start = ((), (), s32[]{:S(2)}) async-start(), calls=%async_computation.15 | async-start | bytes 1622016 | tf_op jit(solution)/shard_map/all_gather | solution.py:115
  312.1 179.9 %all-gather.27.cloned.1.call-start = ((), (), s32[]{:S(2)}) async-start(), calls=%async_computation.11 | async-start | bytes 1622016 | tf_op jit(solution)/shard_map/all_gather | solution.py:114
  312.7 206.0 %all-gather.25.cloned.1.call-start = ((), (), s32[]{:S(2)}) async-start(), calls=%async_computation.10 | async-start | bytes 1622016 | tf_op jit(solution)/shard_map/all_gather | solution.py:113
  315.5 25.5 %copy-start.9 = (bf16[128,2048]{1,0:T(8,128)(2,1)S(1)}, bf16[128,2048]{1,0:T(8,128)(2,1)}, u32[]{:S(2)}) copy-start(bf16[128,2048]{1,0:T(8,128)(2,1)} %copy-done.8) | copy-start | bytes 1572868
  315.5 17.6 %all-to-all-start.3 = ((bf16[128,8,256]{0,2,1:T(8,128)(2,1)}), bf16[128,8,256]{0,2,1:T(8,128)(2,1)S(1)}, u32[]{:S(2)}, u32[]{:S(2)}) async-start(bf16[128,8,256]{0,2,1:T(8,128)(2,1)} %bitcast.8), calls=%async_computation.3 | async-start | bytes 1048576 | tf_op jit(solution)/shard_map/all_to_all | solution.py:109
  321.2 41.5 %copy-start.7 = (bf16[128,2048]{1,0:T(8,128)(2,1)S(1)}, bf16[128,2048]{1,0:T(8,128)(2,1)}, u32[]{:S(2)}) copy-start(bf16[128,2048]{1,0:T(8,128)(2,1)} %param.19) | copy-start | bytes 1572868
  333.0 33.3 %all-to-all-start.2 = ((bf16[128,8,256]{2,0,1:T(8,128)(2,1)}), bf16[128,8,256]{2,0,1:T(8,128)(2,1)S(1)}, u32[]{:S(2)}, u32[]{:S(2)}) async-start(bf16[128,8,256]{2,0,1:T(8,128)(2,1)} %bitcast.59), calls=%async_computation.2 | async-start | bytes 1048576 | tf_op jit(solution)/shard_map/all_to_all | solution.py:108
  339.9 205.2 %all-gather.29.cloned.1.call-start = ((), (), s32[]{:S(2)}) async-start(), calls=%async_computation.12 | async-start | bytes 1622016 | tf_op jit(solution)/shard_map/all_gather | solution.py:115
  362.6 39.0 %copy-start.16 = (f32[256,704]{0,1:T(8,128)S(1)}, f32[256,704]{0,1:T(8,128)}, u32[]{:S(2)}) copy-start(f32[256,704]{0,1:T(8,128)} %param.34) | copy-start | bytes 2162692
  366.3 66.2 %all-to-all-start = ((bf16[128,8,256]{2,0,1:T(8,128)(2,1)}), bf16[128,8,256]{2,0,1:T(8,128)(2,1)S(1)}, u32[]{:S(2)}, u32[]{:S(2)}) async-start(bf16[128,8,256]{2,0,1:T(8,128)(2,1)} %bitcast.61), calls=%async_computation | async-start | bytes 1048576 | tf_op jit(solution)/shard_map/all_to_all | solution.py:108
  404.4 61.1 %copy-start.17 = (f32[704,256]{1,0:T(8,128)S(1)}, f32[704,256]{1,0:T(8,128)}, u32[]{:S(2)}) copy-start(f32[704,256]{1,0:T(8,128)} %param.35) | copy-start | bytes 2162692
  432.6 59.4 %copy-start.18 = (f32[256,704]{0,1:T(8,128)S(1)}, f32[256,704]{0,1:T(8,128)}, u32[]{:S(2)}) copy-start(f32[256,704]{0,1:T(8,128)} %param.31) | copy-start | bytes 2162692
  432.6 88.8 %all-to-all-start.1 = ((bf16[128,8,256]{2,0,1:T(8,128)(2,1)}), bf16[128,8,256]{2,0,1:T(8,128)(2,1)S(1)}, u32[]{:S(2)}, u32[]{:S(2)}) async-start(bf16[128,8,256]{2,0,1:T(8,128)(2,1)} %bitcast.60), calls=%async_computation.1 | async-start | bytes 1048576 | tf_op jit(solution)/shard_map/all_to_all | solution.py:109
  468.3 50.4 %copy-start.19 = (f32[256,704]{0,1:T(8,128)S(1)}, f32[256,704]{0,1:T(8,128)}, u32[]{:S(2)}) copy-start(f32[256,704]{0,1:T(8,128)} %param.30) | copy-start | bytes 2162692
  492.0 53.1 %copy-start.20 = (f32[704,256]{1,0:T(8,128)S(1)}, f32[704,256]{1,0:T(8,128)}, u32[]{:S(2)}) copy-start(f32[704,256]{1,0:T(8,128)} %param.32) | copy-start | bytes 2162692
Sparse Core Ops, SparseCore 0:
  9.6 37.1 all-gather.18
  48.4 35.2 all-gather.22
  85.3 35.2 all-gather.12
  122.0 35.2 all-gather.20
  158.7 35.2 all-gather.14
  195.4 35.2 all-gather.16
  236.8 51.4 all-reduce.6
  310.2 52.4 all-reduce.4
  364.2 37.4 all-gather.32
  403.7 25.9 all-gather.30
  431.8 33.6 all-gather.34
  467.0 24.9 all-gather.26
  493.6 24.9 all-gather.24
  520.1 24.9 all-gather.28
where the time goes:
time: 556 us; the launch traced here: 554 us
  waiting for transfers between devices  434 us (78%)
  matrix products  63.4 us (11%)
  starting transfers between devices  22.5 us (4%)
  other arithmetic  14.7 us (3%)
  between operations  14.2 us (3%)
  local copies, waits for them, and re-layouts  5.63 us (1%)
    psum x2, waiting for transfers between devices, block_forward(): lax.psum(jnp.dot(hidden, w_down, preferred_element_type=jnp.float32).asty...  65.5 us
    all_gather x2, waiting for transfers between devices, collect(): lax.all_gather(hidden, 'fs', axis=0, tiled=True)  53.1 us
    all_gather x2, waiting for transfers between devices, collect(): lax.all_gather(up_grad, 'fs', axis=0, tiled=True)  51.4 us
    all_gather x2, waiting for transfers between devices, collect(): lax.all_gather(gate_grad, 'fs', axis=0, tiled=True)  49 us
    all_gather x1, waiting for transfers between devices, per_device(): lax.all_gather(down_first, 'fs', axis=1, tiled=True)  36.7 us
    all_gather x1, waiting for transfers between devices, per_device(): lax.all_gather(gate_second, 'fs', axis=0, tiled=True)  33.9 us
    all_gather x1, waiting for transfers between devices, per_device(): lax.all_gather(gate_first, 'fs', axis=0, tiled=True)  33.4 us
    all_gather x1, waiting for transfers between devices, per_device(): lax.all_gather(down_second, 'fs', axis=1, tiled=True)  33.4 us
  transfers between devices with their start and end apart: 18, of which 15 were waited for; matrix products, arithmetic and copies ran while one was open for 9% of the time, Pallas kernels for 0%

commit v1 on v0

--- a/solution.py
+++ b/solution.py
@@ -4,6 +4,11 @@
 from jax.sharding import PartitionSpec as P
 
 norm_eps = 1e-06
+
+
+def summed_here(x, mesh_axis):
+    pieces = lax.all_gather(x, mesh_axis)
+    return jnp.sum(pieces, axis=0)
 
 
 def normalize(values, gain_vector):
@@ -19,7 +24,7 @@
     gate_pre = jnp.dot(normed, w_gate, preferred_element_type=jnp.float32)
     up_pre = jnp.dot(normed, w_up, preferred_element_type=jnp.float32)
     hidden = (jax.nn.silu(gate_pre) * up_pre).astype(jnp.bfloat16)
-    branch = lax.psum(
+    branch = summed_here(
         jnp.dot(hidden, w_down, preferred_element_type=jnp.float32).astype(jnp.bfloat16), "tp"
     ).astype(jnp.float32)
     return (widened + 0.5 * branch).astype(jnp.bfloat16)

time: 556 us -> 592 us (1.065)
  waiting for transfers between devices: 434 us -> 464 us
    all_gather x0 -> x2, waiting for transfers between devices: none -> 42.8 us  [summed_here(): pieces = lax.all_gather(x, mesh_axis)]
    all_to_all x2, waiting for transfers between devices: 11 us -> 0.01 us  [collect(): lax.all_to_all(cotan_rows, 'fs', split_axis=1, concat_axis=0, tiled=True)]
    all_gather x1, waiting for transfers between devices: 33.4 us -> 26.6 us  [per_device(): lax.all_gather(gate_first, 'fs', axis=0, tiled=True)]
    all_gather x1, waiting for transfers between devices: 26.7 us -> 33 us  [per_device(): lax.all_gather(up_first, 'fs', axis=0, tiled=True)]
  transfers between devices with their start and end apart: 18 -> 20, of which waited for: 15 -> 16; matrix products, arithmetic and copies ran while one was open for 9% -> 14% of each run, Pallas kernels for 0% -> 0%
where the time goes in v1:
time: 592 us; the launch traced here: 589 us
  waiting for transfers between devices  464 us (78%)
  matrix products  64.7 us (11%)
  starting transfers between devices  22 us (4%)
  other arithmetic  17.4 us (3%)
  between operations  14.2 us (2%)
  local copies, waits for them, and re-layouts  7.44 us (1%)
    psum x2, waiting for transfers between devices, block_backward(): lax.psum(partial_value.astype(jnp.bfloat16), 'tp').astype(jnp.float32)  63.8 us
    all_gather x2, waiting for transfers between devices, collect(): lax.all_gather(hidden, 'fs', axis=0, tiled=True)  52.9 us
    all_gather x2, waiting for transfers between devices, collect(): lax.all_gather(gate_grad, 'fs', axis=0, tiled=True)  51.1 us
    all_gather x2, waiting for transfers between devices, collect(): lax.all_gather(up_grad, 'fs', axis=0, tiled=True)  49.1 us
    all_gather x2, waiting for transfers between devices, summed_here(): pieces = lax.all_gather(x, mesh_axis)  42.8 us
    all_gather x1, waiting for transfers between devices, per_device(): lax.all_gather(down_first, 'fs', axis=1, tiled=True)  36.7 us
    all_gather x1, waiting for transfers between devices, per_device(): lax.all_gather(down_second, 'fs', axis=1, tiled=True)  33.8 us
    all_gather x1, waiting for transfers between devices, per_device(): lax.all_gather(up_second, 'fs', axis=0, tiled=True)  33.4 us
  transfers between devices with their start and end apart: 20, of which 16 were waited for; matrix products, arithmetic and copies ran while one was open for 14% of the time, Pallas kernels for 0%

profile of v1, /device:TPU:9, one launch (start us, length us, event | category | flops | bytes accessed | tf_op | source)
XLA Modules:
  0.0 589.2 jit_solution(17959031993778191498)
XLA Ops:
  13.1 33.8 %all-gather.27.cloned.1.call-done = bf16[704,2048]{1,0:T(8,128)(2,1)} async-done(((bf16[704,256]{1,0:T(8,128)(2,1)}), bf16[704,2048]{1,0:T(8,128)(2,1)}) %all-gather.27.cloned.1.call-update) | async-done | bytes 2883600 | tf_op jit(solution)/shard_map/all_gather | solution.py:103
  46.9 3.5 convolution_multiply_fusion.3
  50.3 33.4 %all-gather.23.cloned.1.call-done = bf16[2048,704]{0,1:T(8,128)(2,1)} async-done(((bf16[256,704]{0,1:T(8,128)(2,1)}), bf16[2048,704]{0,1:T(8,128)(2,1)}) %all-gather.23.cloned.1.call-update) | async-done | bytes 2883600 | tf_op jit(solution)/shard_map/all_gather | solution.py:98
  83.7 3.5 fusion.59
  87.2 33.4 %all-gather.25.cloned.1.call-done = bf16[2048,704]{0,1:T(8,128)(2,1)} async-done(((bf16[256,704]{0,1:T(8,128)(2,1)}), bf16[2048,704]{0,1:T(8,128)(2,1)}) %all-gather.25.cloned.1.call-update) | async-done | bytes 2883600 | tf_op jit(solution)/shard_map/all_gather | solution.py:99
  120.6 3.8 multiply_convert_fusion
  124.4 2.5 fusion.60
  126.9 3.7 fusion
  130.7 26.6 %all-gather.17.cloned.1.call-done = bf16[2048,704]{0,1:T(8,128)(2,1)} async-done(((bf16[256,704]{0,1:T(8,128)(2,1)}), bf16[2048,704]{0,1:T(8,128)(2,1)}) %all-gather.17.cloned.1.call-update) | async-done | bytes 2883600 | tf_op jit(solution)/shard_map/all_gather | solution.py:96
  157.3 3.7 fusion.54
  161.0 33.0 %all-gather.19.cloned.1.call-done = bf16[2048,704]{0,1:T(8,128)(2,1)} async-done(((bf16[256,704]{0,1:T(8,128)(2,1)}), bf16[2048,704]{0,1:T(8,128)(2,1)}) %all-gather.19.cloned.1.call-update) | async-done | bytes 2883600 | tf_op jit(solution)/shard_map/all_gather | solution.py:97
  194.0 36.7 %all-gather.21.cloned.1.call-done = bf16[704,2048]{1,0:T(8,128)(2,1)} async-done(((bf16[704,256]{1,0:T(8,128)(2,1)}), bf16[704,2048]{1,0:T(8,128)(2,1)}) %all-gather.21.cloned.1.call-update) | async-done | bytes 2883600 | tf_op jit(solution)/shard_map/all_gather | solution.py:102
  230.7 6.0 %convolution_convert_fusion.1 = bf16[128,2048]{1,0:T(8,128)(2,1)} fusion(bf16[704,2048]{1,0:T(8,128)(2,1)} %all-gather.21.cloned.1.call-done, bf16[2048,704]{0,1:T(8,128)(2,1)} %all-gather.19.cloned.1.call-done, f32[128,704]{0,1:T(8,128)} %fusion.54, bf16[128,2048]{1,0:T(8,128)(2,1)} %param.18, f32[2048]{0:T(1024)S(1)} %copy-done.23, f32[128]{0:T(128)S(1)} %add_rsqrt_fusion.3), kind=kOutput, calls=%fused_computation.5 | convolution fusion | flops 740048896 | bytes 7184896 | tf_op jit(solution)/shard_map/dot_general | solution.py:28
  239.0 3.5 fusion.61
  242.5 35.8 %all-reduce.3.cloned.1.call-done = bf16[128,2048]{1,0:T(8,128)(2,1)} async-done(((bf16[128,2048]{1,0:T(8,128)(2,1)}), bf16[128,2048]{1,0:T(8,128)(2,1)}) %all-reduce.3.cloned.1.call-update) | async-done | bytes 524304 | tf_op jit(solution)/shard_map/psum | solution.py:52
  278.3 1.5 fusion.13
  279.9 1.8 fusion.17
  283.4 1.6 multiply_convert_fusion.1
  285.0 3.6 fusion.62
  288.6 3.8 fusion.1
  296.3 2.0 copy.33
  298.3 5.8 all-to-all-start.3
  305.0 11.3 %all-gather.41.cloned.1.call-done = bf16[512,2048]{1,0:T(8,128)(2,1)} async-done(((bf16[128,2048]{1,0:T(8,128)(2,1)}), bf16[512,2048]{1,0:T(8,128)(2,1)}) %all-gather.41.cloned.1.call-update) | async-done | bytes 2097168 | tf_op jit(solution)/shard_map/all_gather | solution.py:10
  316.3 2.9 reduce_sum.79
  319.2 1.5 fusion.30
  320.8 1.7 fusion.50
  322.5 5.6 all-to-all-start.2
  328.1 5.9 %convolution_convert_fusion = bf16[128,2048]{1,0:T(8,128)(2,1)} fusion(bf16[704,2048]{1,0:T(8,128)(2,1)} %all-gather.27.cloned.1.call-done, bf16[2048,704]{0,1:T(8,128)(2,1)} %all-gather.25.cloned.1.call-done, f32[128,704]{0,1:T(8,128)} %fusion.50, bf16[128,2048]{1,0:T(8,128)(2,1)S(1)} %get-tuple-element.10, f32[2048]{0:T(1024)S(1)} %copy-done.22, ...), kind=kOutput, calls=%fused_computation.4 | convolution fusion | flops 740048896 | bytes 7184896 | tf_op jit(solution)/shard_map/dot_general | solution.py:28
  334.9 1.2 copy.34
  337.0 28.0 %all-reduce.5.cloned.1.call-done = bf16[128,2048]{1,0:T(8,128)(2,1)} async-done(((bf16[128,2048]{1,0:T(8,128)(2,1)}), bf16[128,2048]{1,0:T(8,128)(2,1)}) %all-reduce.5.cloned.1.call-update) | async-done | bytes 524304 | tf_op jit(solution)/shard_map/psum | solution.py:52
  365.0 1.4 fusion.20
  366.3 6.0 %all-to-all-start = ((bf16[128,8,256]{2,0,1:T(8,128)(2,1)}), bf16[128,8,256]{2,0,1:T(8,128)(2,1)S(1)}, u32[]{:S(2)}, u32[]{:S(2)}) async-start(bf16[128,8,256]{2,0,1:T(8,128)(2,1)} %bitcast.63), calls=%async_computation | async-start | bytes 1048576 | tf_op jit(solution)/shard_map/all_to_all | solution.py:113
  372.3 2.3 fusion.24
  374.6 27.4 %all-gather.35.cloned.1.call-done = bf16[1024,704]{0,1:T(8,128)(2,1)} async-done(((bf16[128,704]{0,1:T(8,128)(2,1)}), bf16[1024,704]{0,1:T(8,128)(2,1)}) %all-gather.35.cloned.1.call-update) | async-done | bytes 1441808 | tf_op jit(solution)/shard_map/all_gather | solution.py:118
  401.9 2.9 convolution_add_fusion.3
  404.9 25.3 %all-gather.37.cloned.1.call-done = bf16[1024,704]{0,1:T(8,128)(2,1)} async-done(((bf16[128,704]{0,1:T(8,128)(2,1)}), bf16[1024,704]{0,1:T(8,128)(2,1)}) %all-gather.37.cloned.1.call-update) | async-done | bytes 1441808 | tf_op jit(solution)/shard_map/all_gather | solution.py:119
  430.2 2.8 convolution_add_fusion.2
  433.0 3.8 all-to-all-start.1
  436.8 29.2 %all-gather.39.cloned.1.call-done = bf16[1024,704]{0,1:T(8,128)(2,1)} async-done(((bf16[128,704]{0,1:T(8,128)(2,1)}), bf16[1024,704]{0,1:T(8,128)(2,1)}) %all-gather.39.cloned.1.call-update) | async-done | bytes 1441808 | tf_op jit(solution)/shard_map/all_gather | solution.py:120
  465.9 2.9 fusion.8
  468.9 23.7 %all-gather.29.cloned.1.call-done = bf16[1024,704]{0,1:T(8,128)(2,1)} async-done(((bf16[128,704]{0,1:T(8,128)(2,1)}), bf16[1024,704]{0,1:T(8,128)(2,1)}) %all-gather.29.cloned.1.call-update) | async-done | bytes 1441808 | tf_op jit(solution)/shard_map/all_gather | solution.py:118
  492.6 2.8 convolution_add_fusion.5
  495.3 23.7 %all-gather.31.cloned.1.call-done = bf16[1024,704]{0,1:T(8,128)(2,1)} async-done(((bf16[128,704]{0,1:T(8,128)(2,1)}), bf16[1024,704]{0,1:T(8,128)(2,1)}) %all-gather.31.cloned.1.call-update) | async-done | bytes 1441808 | tf_op jit(solution)/shard_map/all_gather | solution.py:119
  519.0 2.8 convolution_add_fusion.4
  521.8 23.7 %all-gather.33.cloned.1.call-done = bf16[1024,704]{0,1:T(8,128)(2,1)} async-done(((bf16[128,704]{0,1:T(8,128)(2,1)}), bf16[1024,704]{0,1:T(8,128)(2,1)}) %all-gather.33.cloned.1.call-update) | async-done | bytes 1441808 | tf_op jit(solution)/shard_map/all_gather | solution.py:120
  545.5 2.8 fusion.9
  548.3 31.4 %all-gather.43.cloned.1.call-done = bf16[512,2048]{1,0:T(8,128)(2,1)} async-done(((bf16[128,2048]{1,0:T(8,128)(2,1)}), bf16[512,2048]{1,0:T(8,128)(2,1)}) %all-gather.43.cloned.1.call-update) | async-done | bytes 2097168 | tf_op jit(solution)/shard_map/all_gather | solution.py:10
  579.7 2.0 reduce_sum.81
  (100 shorter events, 17.1 us)
Async XLA Ops:
  7.2 5.3 copy-start.5
  7.2 5.5 copy-start.4
  7.2 5.7 copy-start.22
  7.2 39.7 %copy-start.14 = (bf16[128,2048]{1,0:T(8,128)(2,1)S(1)}, bf16[128,2048]{1,0:T(8,128)(2,1)}, u32[]{:S(2)}) copy-start(bf16[128,2048]{1,0:T(8,128)(2,1)} %param.21) | copy-start | bytes 1572868
  7.2 39.6 %all-gather.27.cloned.1.call-start = ((), (), s32[]{:S(2)}) async-start(), calls=%async_computation.9 | async-start | bytes 3244032 | tf_op jit(solution)/shard_map/all_gather | solution.py:103
  8.0 75.8 %all-gather.23.cloned.1.call-start = ((), (), s32[]{:S(2)}) async-start(), calls=%async_computation.7 | async-start | bytes 3244032 | tf_op jit(solution)/shard_map/all_gather | solution.py:98
  8.7 111.9 %all-gather.25.cloned.1.call-start = ((), (), s32[]{:S(2)}) async-start(), calls=%async_computation.8 | async-start | bytes 3244032 | tf_op jit(solution)/shard_map/all_gather | solution.py:99
  9.4 147.8 %all-gather.17.cloned.1.call-start = ((), (), s32[]{:S(2)}) async-start(), calls=%async_computation.4 | async-start | bytes 3244032 | tf_op jit(solution)/shard_map/all_gather | solution.py:96
  10.0 184.0 %all-gather.19.cloned.1.call-start = ((), (), s32[]{:S(2)}) async-start(), calls=%async_computation.5 | async-start | bytes 3244032 | tf_op jit(solution)/shard_map/all_gather | solution.py:97
  10.6 220.1 %all-gather.21.cloned.1.call-start = ((), (), s32[]{:S(2)}) async-start(), calls=%async_computation.6 | async-start | bytes 3244032 | tf_op jit(solution)/shard_map/all_gather | solution.py:102
  11.2 267.2 %all-reduce.3.cloned.1.call-start = ((), (), s32[]{:S(2)}) async-start(), calls=%async_computation.10 | async-start | bytes 1048576 | tf_op jit(solution)/shard_map/psum | solution.py:52
  13.1 70.7 %copy-start.9 = (bf16[128,2048]{1,0:T(8,128)(2,1)}, bf16[128,2048]{1,0:T(8,128)(2,1)S(1)}, u32[]{:S(2)}) copy-start(bf16[128,2048]{1,0:T(8,128)(2,1)S(1)} %fusion.12) | copy-start | bytes 1572868
  87.2 37.2 %copy-start = (bf16[2048,704]{0,1:T(8,128)(2,1)S(1)}, bf16[2048,704]{0,1:T(8,128)(2,1)}, u32[]{:S(2)}) copy-start(bf16[2048,704]{0,1:T(8,128)(2,1)} %all-gather.23.cloned.1.call-done) | copy-start | bytes 8650756
  126.9 30.4 %copy-start.23 = (f32[2048]{0:T(1024)S(1)}, f32[2048]{0:T(1024)}, u32[]{:S(2)}) copy-start(f32[2048]{0:T(1024)} %param.22) | copy-start | bytes 24580
  130.7 185.7 %all-gather.41.cloned.1.call-start = ((), (), s32[]{:S(2)}) async-start(), calls=%async_computation.18 | async-start | bytes 2621440 | tf_op jit(solution)/shard_map/all_gather | solution.py:10
  236.7 128.2 %all-reduce.5.cloned.1.call-start = ((), (), s32[]{:S(2)}) async-start(), calls=%async_computation.11 | async-start | bytes 1048576 | tf_op jit(solution)/shard_map/psum | solution.py:52
  238.2 0.8 copy-start.11
  278.3 4.1 copy-start.2
  279.9 3.5 copy-start.1
  279.9 3.5 copy-start.12
  279.9 3.5 copy-start.21
  281.7 0.8 copy-start.7
  285.0 3.6 copy-start.15
  285.0 3.6 copy-start.16
  292.4 11.7 %copy-start.10 = (bf16[128,2048]{1,0:T(8,128)(2,1)S(1)}, bf16[128,2048]{1,0:T(8,128)(2,1)}, u32[]{:S(2)}) copy-start(bf16[128,2048]{1,0:T(8,128)(2,1)} %copy-done.9) | copy-start | bytes 1572868
  292.4 109.5 %all-gather.35.cloned.1.call-start = ((), (), s32[]{:S(2)}) async-start(), calls=%async_computation.15 | async-start | bytes 1622016 | tf_op jit(solution)/shard_map/all_gather | solution.py:118
  293.0 137.2 %all-gather.37.cloned.1.call-start = ((), (), s32[]{:S(2)}) async-start(), calls=%async_computation.16 | async-start | bytes 1622016 | tf_op jit(solution)/shard_map/all_gather | solution.py:119
  293.8 172.2 %all-gather.39.cloned.1.call-start = ((), (), s32[]{:S(2)}) async-start(), calls=%async_computation.17 | async-start | bytes 1622016 | tf_op jit(solution)/shard_map/all_gather | solution.py:120
  294.3 198.2 %all-gather.29.cloned.1.call-start = ((), (), s32[]{:S(2)}) async-start(), calls=%async_computation.12 | async-start | bytes 1622016 | tf_op jit(solution)/shard_map/all_gather | solution.py:118
  295.1 223.9 %all-gather.31.cloned.1.call-start = ((), (), s32[]{:S(2)}) async-start(), calls=%async_computation.13 | async-start | bytes 1622016 | tf_op jit(solution)/shard_map/all_gather | solution.py:119
  295.7 249.9 %all-gather.33.cloned.1.call-start = ((), (), s32[]{:S(2)}) async-start(), calls=%async_computation.14 | async-start | bytes 1622016 | tf_op jit(solution)/shard_map/all_gather | solution.py:120
  298.3 24.2 %all-to-all-start.3 = ((bf16[128,8,256]{0,2,1:T(8,128)(2,1)}), bf16[128,8,256]{0,2,1:T(8,128)(2,1)}, u32[]{:S(2)}, u32[]{:S(2)}) async-start(bf16[128,8,256]{0,2,1:T(8,128)(2,1)} %bitcast.74), calls=%async_computation.3 | async-start | bytes 1048576 | tf_op jit(solution)/shard_map/all_to_all | solution.py:114
  320.7 261.0 %copy-start.3 = (bf16[128,2048]{1,0:T(8,128)(2,1)}, bf16[128,2048]{1,0:T(8,128)(2,1)S(1)}, u32[]{:S(2)}) copy-start(bf16[128,2048]{1,0:T(8,128)(2,1)S(1)} %get-tuple-element.10) | copy-start | bytes 1572868
  322.5 43.8 %all-to-all-start.2 = ((bf16[128,8,256]{2,0,1:T(8,128)(2,1)}), bf16[128,8,256]{2,0,1:T(8,128)(2,1)S(1)}, u32[]{:S(2)}, u32[]{:S(2)}) async-start(bf16[128,8,256]{2,0,1:T(8,128)(2,1)} %bitcast.73), calls=%async_computation.2 | async-start | bytes 1048576 | tf_op jit(solution)/shard_map/all_to_all | solution.py:113
  328.1 6.0 %copy-start.13 = (bf16[128,2048]{1,0:T(8,128)(2,1)S(1)}, bf16[128,2048]{1,0:T(8,128)(2,1)}, u32[]{:S(2)}) copy-start(bf16[128,2048]{1,0:T(8,128)(2,1)} %copy-done.11) | copy-start | bytes 1572868
  328.1 251.6 %all-gather.43.cloned.1.call-start = ((), (), s32[]{:S(2)}) async-start(), calls=%async_computation.19 | async-start | bytes 2621440 | tf_op jit(solution)/shard_map/all_gather | solution.py:10
  334.0 2.1 copy-start.8
  334.0 30.9 %copy-start.6 = (bf16[128,2048]{1,0:T(8,128)(2,1)S(1)}, bf16[128,2048]{1,0:T(8,128)(2,1)}, u32[]{:S(2)}) copy-start(bf16[128,2048]{1,0:T(8,128)(2,1)} %param.19) | copy-start | bytes 1572868
  366.3 66.6 %all-to-all-start = ((bf16[128,8,256]{2,0,1:T(8,128)(2,1)}), bf16[128,8,256]{2,0,1:T(8,128)(2,1)S(1)}, u32[]{:S(2)}, u32[]{:S(2)}) async-start(bf16[128,8,256]{2,0,1:T(8,128)(2,1)} %bitcast.63), calls=%async_computation | async-start | bytes 1048576 | tf_op jit(solution)/shard_map/all_to_all | solution.py:113
  374.5 55.7 %copy-start.17 = (f32[256,704]{0,1:T(8,128)S(1)}, f32[256,704]{0,1:T(8,128)}, u32[]{:S(2)}) copy-start(f32[256,704]{0,1:T(8,128)} %param.34) | copy-start | bytes 2162692
  433.0 59.6 %copy-start.18 = (f32[256,704]{0,1:T(8,128)S(1)}, f32[256,704]{0,1:T(8,128)}, u32[]{:S(2)}) copy-start(f32[256,704]{0,1:T(8,128)} %param.30) | copy-start | bytes 2162692
  433.0 88.8 %all-to-all-start.1 = ((bf16[128,8,256]{2,0,1:T(8,128)(2,1)}), bf16[128,8,256]{2,0,1:T(8,128)(2,1)S(1)}, u32[]{:S(2)}, u32[]{:S(2)}) async-start(bf16[128,8,256]{2,0,1:T(8,128)(2,1)} %bitcast.62), calls=%async_computation.1 | async-start | bytes 1048576 | tf_op jit(solution)/shard_map/all_to_all | solution.py:114
  468.9 50.2 %copy-start.19 = (f32[256,704]{0,1:T(8,128)S(1)}, f32[256,704]{0,1:T(8,128)}, u32[]{:S(2)}) copy-start(f32[256,704]{0,1:T(8,128)} %param.31) | copy-start | bytes 2162692
  495.3 50.2 %copy-start.20 = (f32[704,256]{1,0:T(8,128)S(1)}, f32[704,256]{1,0:T(8,128)}, u32[]{:S(2)}) copy-start(f32[704,256]{1,0:T(8,128)} %param.32) | copy-start | bytes 2162692
Sparse Core Ops, SparseCore 0:
  9.6 37.1 all-gather.26
  48.4 35.2 all-gather.22
  85.3 35.2 all-gather.24
  122.0 35.2 all-gather.16
  158.7 35.2 all-gather.18
  195.4 35.2 all-gather.20
  234.3 44.0 all-reduce.2
  280.8 35.5 all-gather.40
  319.9 45.0 all-reduce.4
  366.4 35.4 all-gather.34
  403.5 26.6 all-gather.36
  432.2 33.6 all-gather.38
  467.5 24.9 all-gather.28
  494.0 24.9 all-gather.30
  520.5 24.9 all-gather.32
  547.8 31.8 all-gather.42
